TPU v7x, 32 devices: a whole 2x2x4 slice. The times are simulated.
32 devices in a mesh: grp: 2 (over y), kv: 4 (over z), tp: 4 (over x, core).
Axes of the slice: x: 2, y: 2, z: 4, core: 2. Of those that a mesh axis runs over, the one named last changes fastest.
Arguments:
- tokens: bfloat16 [8, 3, 4096], P(('grp', 'kv')), parts along dimension 0, may hold values from -6 to 6
- input_norm_scale: float32 [4096], replicated, may hold values from 0.1 to 1.9
- head_input_matrix: bfloat16 [4096, 8192], P('kv', 'tp'), may hold values from -0.09375 to 0.09375
- output_gate_matrix: bfloat16 [4096, 8192], P('kv', 'tp'), may hold values from -0.09375 to 0.09375
- group_input_matrix: bfloat16 [4096, 512], P('kv', 'tp'), may hold values from -0.09375 to 0.09375
- group_readout_matrix: bfloat16 [4096, 512], P('kv', 'tp'), may hold values from -0.09375 to 0.09375
- step_size_matrix: bfloat16 [4096, 128], P(None, 'tp'), may hold values from -0.09375 to 0.09375
- step_size_bias: float32 [128], P('tp'), may hold values from -4 to -1
- log_decay_rate: float32 [128], P('tp'), may hold values from -4.6 to 2
- direct_path_weight: float32 [128], P('tp'), may hold values from 0.1 to 1.9
- convolution_tap_weight: bfloat16 [4, 8, 1152], P(None, 'tp'), may hold values from -3 to 3
- convolution_history_rows: bfloat16 [8, 6, 8, 1152], P(('grp', 'kv'), None, 'tp'), parts along dimension 0, may hold values from -6 to 6
- per_proposal_states: float32 [8, 3, 128, 64, 64], P(('grp', 'kv'), None, 'tp'), parts along dimension 0, may hold values from -4 to 4
- accepted: int32 [8], P(('grp', 'kv')), parts along dimension 0, may hold values from 1 to 3
- proposal_extra_decay: float32 [8, 3, 128], P(('grp', 'kv'), None, 'tp'), parts along dimension 0, may hold values from -0.69 to 0
- group_norm_scale: float32 [8192], P('tp'), may hold values from 0.1 to 1.9
- output_projection_matrix: bfloat16 [8192, 4096], P('tp', 'kv'), may hold values from -0.0625 to 0.0625
Outputs:
- mixed: bfloat16 [8, 3, 4096], P(('grp', 'tp'), None, 'kv'), parts along dimension 0
- new_states: float32 [8, 3, 128, 64, 64], P(('grp', 'kv'), None, 'tp'), parts along dimension 0
- new_tail: bfloat16 [8, 6, 8, 1152], P(('grp', 'kv'), None, 'tp'), parts along dimension 0
There are 2 independent parts, one for each index of `grp`. A program takes and returns all parts, laid end to end along the dimension named above; an argument that names none is the same for every part. Nothing has to cross between parts.
All inputs are finite; a program needn't handle non-finite values.
Results may differ from a plain program's by a relative error of at most 0.015.
Values may be sent and summed in bfloat16 or wider, within the bound.
A program may use at most 64 MiB of HBM per device.

v0:
```python
import jax
import jax.numpy as jnp
from jax import lax
from jax.sharding import PartitionSpec as P

epsilon = 1e-06


def rms_scale(values):
    return lax.rsqrt(jnp.mean(values * values, axis=-1, keepdims=True) + epsilon)


def causal_states(log_decay_factor, head_step_size, ssm_inputs, inject, start_state):
    cumulative = jnp.cumsum(log_decay_factor, axis=1)
    length = log_decay_factor.shape[1]
    lower = (jnp.arange(length)[:, None] >= jnp.arange(length)[None, :])[None, :, :, None]
    spread = cumulative[:, :, None, :] - cumulative[:, None, :, :]
    factors = jnp.where(lower, jnp.exp(jnp.where(lower, spread, 0.0)), 0.0)
    mixing = factors * head_step_size[:, None, :, :]
    carried = jnp.exp(cumulative)[..., None, None] * start_state[:, None]
    return carried + jnp.einsum("sjih,sihp,sihn->sjhpn", mixing, ssm_inputs, inject)


def combine_head_outputs(
    incoming_token_rows,
    gate_portion,
    unactivated_step,
    step_size_bias,
    log_decay_rate,
    direct_path_weight,
    convolution_tap_weight,
    convolution_history_rows,
    per_proposal_states,
    accepted,
    proposal_extra_decay,
    group_norm_scale,
):
    sequences, proposals, group_count, group_width = incoming_token_rows.shape
    head_count = step_size_bias.shape[0]
    head_dim = per_proposal_states.shape[3]
    state_size = per_proposal_states.shape[4]
    per_group = head_count // group_count
    group_inner = per_group * head_dim
    tap_count = convolution_tap_weight.shape[0]
    offsets = accepted[:, None] + jnp.arange(tap_count - 1, dtype=jnp.int32)[None, :]
    context = jnp.take_along_axis(convolution_history_rows, offsets[:, :, None, None], axis=1)
    convolution_span = jnp.concatenate([context, incoming_token_rows], axis=1)
    widened = convolution_span.astype(jnp.float32)
    convolved = jnp.zeros((sequences, proposals, group_count, group_width), jnp.float32)
    for conv_tap in range(tap_count):
        convolved = convolved + widened[
            :, conv_tap : conv_tap + proposals
        ] * convolution_tap_weight[conv_tap].astype(jnp.float32)
    activated = jax.nn.silu(convolved)
    ssm_inputs = activated[..., :group_inner].reshape(sequences, proposals, head_count, head_dim)
    inject = jnp.repeat(activated[..., group_inner : group_inner + state_size], per_group, axis=2)
    readout = jnp.repeat(activated[..., group_inner + state_size :], per_group, axis=2)
    head_step_size = jax.nn.softplus(unactivated_step + step_size_bias)
    log_decay_factor = proposal_extra_decay - jnp.exp(log_decay_rate) * head_step_size
    chosen = (accepted - 1)[:, None, None, None, None]
    start_state = jnp.take_along_axis(per_proposal_states, chosen, axis=1)[:, 0]
    running_state_rows = causal_states(
        log_decay_factor, head_step_size, ssm_inputs, inject, start_state
    )
    response = (
        jnp.einsum("sjhn,sjhpn->sjhp", readout, running_state_rows)
        + direct_path_weight[:, None] * ssm_inputs
    )
    gate_raw = gate_portion.astype(jnp.float32).reshape(sequences, proposals, head_count, head_dim)
    gate_applied_output = (response * jax.nn.silu(gate_raw)).reshape(
        sequences, proposals, group_count, group_inner
    )
    scaled = (
        gate_applied_output
        * rms_scale(gate_applied_output)
        * group_norm_scale.reshape(group_count, group_inner)
    )
    flat_gated = scaled.astype(jnp.bfloat16).reshape(sequences, proposals, head_count * head_dim)
    return (flat_gated, running_state_rows, convolution_span)


def local(
    tokens,
    input_norm_scale,
    head_input_matrix,
    output_gate_matrix,
    group_input_matrix,
    group_readout_matrix,
    step_size_matrix,
    step_size_bias,
    log_decay_rate,
    direct_path_weight,
    convolution_tap_weight,
    convolution_history_rows,
    per_proposal_states,
    accepted,
    proposal_extra_decay,
    group_norm_scale,
    output_projection_matrix,
):
    local_seqs, proposals, width = tokens.shape
    head_local = step_size_bias.shape[0]
    group_local = convolution_tap_weight.shape[1]
    head_dim = per_proposal_states.shape[3]
    state_size = per_proposal_states.shape[4]
    group_inner = head_local // group_local * head_dim
    widened = tokens.astype(jnp.float32)
    normed = (widened * rms_scale(widened) * input_norm_scale).astype(jnp.bfloat16)
    unactivated_step = jnp.einsum(
        "sjd,dh->sjh", normed, step_size_matrix, preferred_element_type=jnp.float32
    )
    pieces = lax.all_to_all(normed, "kv", split_axis=2, concat_axis=0, tiled=True)
    joined = jnp.concatenate(
        [head_input_matrix, group_input_matrix, group_readout_matrix, output_gate_matrix], axis=1
    )
    summed = lax.psum_scatter(
        jnp.einsum("sjd,dc->sjc", pieces, joined, preferred_element_type=jnp.float32),
        "kv",
        scatter_dimension=0,
        tiled=True,
    )
    projected = summed.astype(jnp.bfloat16)
    input_width = head_local * head_dim
    inject_width = group_local * state_size
    part_input = projected[..., :input_width].reshape(
        local_seqs, proposals, group_local, group_inner
    )
    part_inject = projected[..., input_width : input_width + inject_width].reshape(
        local_seqs, proposals, group_local, state_size
    )
    part_readout = projected[
        ..., input_width + inject_width : input_width + 2 * inject_width
    ].reshape(local_seqs, proposals, group_local, state_size)
    gate_portion = projected[..., input_width + 2 * inject_width :]
    incoming_token_rows = jnp.concatenate([part_input, part_inject, part_readout], axis=-1)
    gate_applied_output, running_state_rows, convolution_span = combine_head_outputs(
        incoming_token_rows,
        gate_portion,
        unactivated_step,
        step_size_bias,
        log_decay_rate,
        direct_path_weight,
        convolution_tap_weight,
        convolution_history_rows,
        per_proposal_states,
        accepted,
        proposal_extra_decay,
        group_norm_scale,
    )
    terms = jnp.einsum(
        "sjc,cd->sjd",
        lax.all_gather(gate_applied_output, "kv", axis=0, tiled=True),
        output_projection_matrix,
        preferred_element_type=jnp.float32,
    )
    mixed = lax.psum_scatter(terms.astype(jnp.bfloat16), "tp", scatter_dimension=0, tiled=True)
    return (mixed, running_state_rows, convolution_span)


def solution(mesh):
    return jax.shard_map(
        local,
        mesh=mesh,
        in_specs=(
            P(("grp", "kv"), None, None),
            P(),
            P("kv", "tp"),
            P("kv", "tp"),
            P("kv", "tp"),
            P("kv", "tp"),
            P(None, "tp"),
            P("tp"),
            P("tp"),
            P("tp"),
            P(None, "tp", None),
            P(("grp", "kv"), None, "tp", None),
            P(("grp", "kv"), None, "tp", None, None),
            P(("grp", "kv")),
            P(("grp", "kv"), None, "tp"),
            P("tp"),
            P("tp", "kv"),
        ),
        out_specs=(
            P(("grp", "tp"), None, "kv"),
            P(("grp", "kv"), None, "tp", None, None),
            P(("grp", "kv"), None, "tp", None),
        ),
        check_vma=False,
    )
```

profile of v0, /device:TPU:0, one launch (start us, length us, event | category | flops | bytes accessed | tf_op | source)
XLA Modules:
  0.0 112.8 jit_solution(2285924247131712935)
XLA Ops:
  0.7 0.9 fusion.12
  1.6 0.9 fusion.14
  2.5 2.8 %copy.69 = bf16[1,3,4096]{1,0,2:T(2,128)(2,1)S(1)} copy(bf16[1,3,4096]{2,1,0:T(4,128)(2,1)S(1)} %fusion.14) | data formatting | bytes 49152 | tf_op jit(solution)/shard_map/convert_element_type | solution.py:108
  5.8 22.4 %reduce.15 = bf16[4096,3]{1,0:T(8,128)(2,1)S(1)} reduce(bf16[4096,1,3]{2,1,0:T(2,128)(2,1)S(1)} %bitcast.84, bf16[]{:T(256)} %broadcast.303), dimensions={1}, to_apply=%bitcast.74.reduce_sub_computation | reduce | bytes 49154
  28.3 2.1 %reshape.441 = bf16[4,2,1536]{2,1,0:T(2,128)(2,1)} reshape(bf16[4096,3]{1,0:T(8,128)(2,1)S(1)} %reduce.15) | data formatting | bytes 49152
  30.4 6.3 %all-to-all-start = ((bf16[4,2,1536]{2,1,0:T(2,128)(2,1)}), bf16[4,2,1536]{2,1,0:T(2,128)(2,1)S(1)}, u32[]{:S(2)}, u32[]{:S(2)}) async-start(bf16[4,2,1536]{2,1,0:T(2,128)(2,1)} %reshape.441), calls=%async_computation | async-start | bytes 49152 | tf_op jit(solution)/shard_map/all_to_all | solution.py:112
  39.5 0.8 compare_select_fusion
  40.4 0.7 fusion.23
  41.4 1.3 %fusion.8 = f32[32,64,64]{2,1,0:T(8,128)S(1)} fusion(f32[1,3,32,64,64]{4,3,2,1,0:T(8,128)} %param.29, s32[]{:T(128)} %bitcast.20, pred[]{:T(512)} %bitcast.19), kind=kLoop, calls=%fused_computation.11 | loop fusion | flops 131072 | bytes 1048581 | tf_op jit(solution)/shard_map/jit(take_along_axis)/select_n | solution.py:61
  42.8 1.2 %dynamic-slice.4 = u32[1]{0:T(128)} dynamic-slice(u32[32]{0:T(128)} %constant.86, u32[]{:T(128)S(6)} %add.157), dynamic_slice_sizes={1} | dynamic-slice | bytes 12
  44.0 1.3 %dynamic-slice.6 = u32[1]{0:T(128)} dynamic-slice(u32[32]{0:T(128)} %constant.90, u32[]{:T(128)S(6)} %add.157), dynamic_slice_sizes={1} | dynamic-slice | bytes 12
  45.3 2.1 %reshape.442 = bf16[4096,1,3]{2,1,0:T(2,128)(2,1)S(1)} reshape(bf16[4,2,1536]{2,1,0:T(2,128)(2,1)S(1)} %all-to-all-done) | data formatting | bytes 49152
  47.4 2.0 %copy.70 = bf16[1,3,4096]{2,1,0:T(4,128)(2,1)S(1)} copy(bf16[1,3,4096]{1,0,2:T(2,128)(2,1)S(1)} %bitcast.85) | data formatting | bytes 49152 | tf_op jit(solution)/shard_map/all_to_all | solution.py:112
  49.5 5.0 %fusion = f32[4,3,4352]{2,0,1:T(4,128)S(1)} fusion(bf16[1024,2048]{1,0:T(8,128)(2,1)} %param.20, bf16[1024,128]{1,0:T(8,128)(2,1)} %param.22, bf16[1024,128]{1,0:T(8,128)(2,1)} %param.21, bf16[1024,2048]{1,0:T(8,128)(2,1)} %param.19, bf16[1,3,4,1024]{3,2,1,0:T(4,128)(2,1)S(1)} %all_to_all.14), kind=kOutput, calls=%fused_computation.2 | convolution fusion | flops 142606336 | bytes 9146368 | tf_op jit(solution)/shard_map/sjd,dc->sjc/dot_general | solution.py:117
  54.5 23.6 %all-reduce.3 = bf16[4,3,4352]{2,0,1:T(4,128)(2,1)S(1)} all-reduce(f32[4,3,4352]{2,0,1:T(4,128)S(1)} %fusion), channel_id=2, replica_groups=mesh['grp'=2,'kv'=4,'tp'=4] {'kv'}, use_global_device_ids=true, to_apply=%region_1.0.clone | all-reduce | flops 52224 | bytes 313344
  78.1 0.7 dynamic-slice_convert_fusion
  79.3 0.7 pad_maximum_fusion
  80.4 1.4 %bitcast_add_fusion = f32[1,3,32,64,64]{4,3,1,2,0:T(8,128)S(1)} fusion(bf16[3,32,64,1]{2,0,3,1:T(4,128)(2,1)S(1)} %bitcast.88, f32[32,64,64]{2,1,0:T(8,128)S(1)} %fusion.8, f32[3,32]{0,1:T(8,128)S(1)} %copy.72, f32[3,32,3]{0,2,1:T(4,128)S(1)} %multiply_bitcast_fusion, f32[3,32,64]{2,0,1:T(4,128)S(1)} %copy.73), kind=kOutput, calls=%fused_computation.5 | convolution fusion | flops 3164160 | bytes 2135552 | tf_op jit(solution)/shard_map/sjih,sihp,sihn->sjhpn/dot_general | solution.py:21
  81.8 1.9 %copy.80 = f32[1,3,32,64,64]{4,3,2,1,0:T(8,128)} copy(f32[1,3,32,64,64]{4,3,1,2,0:T(8,128)S(1)} %bitcast_add_fusion) | data formatting | bytes 3145728
  83.7 0.9 fusion.3
  85.2 13.1 %all_gather.3 = bf16[4,3,2048]{2,1,0:T(4,128)(2,1)S(1)} all-gather(bf16[1,3,2048]{2,1,0:T(4,128)(2,1)S(1)} %multiply_convert_fusion), channel_id=1, replica_groups=mesh['grp'=2,'kv'=4,'tp'=4] {'kv'}, dimensions={0}, use_global_device_ids=true | all-gather | bytes 61440 | tf_op jit(solution)/shard_map/all_gather | solution.py:152
  98.4 2.8 %fusion.5 = bf16[4,3,1024]{2,0,1:T(4,128)(2,1)S(1)} fusion(bf16[2048,1024]{1,0:T(8,128)(2,1)} %param.33, bf16[4,3,2048]{2,1,0:T(4,128)(2,1)S(1)} %all_gather.3), kind=kOutput, calls=%fused_computation.8 | convolution fusion | flops 50343936 | bytes 4268032 | tf_op jit(solution)/shard_map/sjc,cd->sjd/dot_general | solution.py:150
  101.2 10.3 %all-reduce.1 = bf16[4,3,1024]{2,1,0:T(4,128)(2,1)S(1)} all-reduce(bf16[4,3,1024]{2,1,0:T(4,128)(2,1)S(1)} %copy.79), channel_id=3, replica_groups=mesh['grp'=2,'kv'=4,'tp'=4] {'tp'}, use_global_device_ids=true, to_apply=%region_5.6.clone | all-reduce | flops 12288 | bytes 49152
  111.5 1.2 %constant_dynamic-slice_fusion = bf16[1,3,1024]{2,1,0:T(4,128)(2,1)} fusion(bf16[4,3,1024]{2,1,0:T(4,128)(2,1)S(1)} %all-reduce.1, u32[]{:T(128)} %bitcast.45), kind=kLoop, calls=%fused_computation.61 | loop fusion | bytes 12292
  (63 shorter events, 4.6 us)
Async XLA Ops:
  0.6 38.8 %copy-start = (bf16[4096,32]{0,1:T(8,128)(2,1)S(1)}, bf16[4096,32]{0,1:T(8,128)(2,1)}, u32[]{:S(2)}) copy-start(bf16[4096,32]{0,1:T(8,128)(2,1)} %param.23) | copy-start | bytes 786436
  0.6 36.8 %copy-start.7 = (bf16[1,6,2,1152]{3,2,1,0:T(2,128)(2,1)S(1)}, bf16[1,6,2,1152]{3,2,1,0:T(2,128)(2,1)}, u32[]{:S(2)}) copy-start(bf16[1,6,2,1152]{3,2,1,0:T(2,128)(2,1)} %param.28) | copy-start | bytes 82948
  0.7 37.5 %copy-start.5 = (bf16[4,2,1152]{2,1,0:T(2,128)(2,1)S(1)}, bf16[4,2,1152]{2,1,0:T(2,128)(2,1)}, u32[]{:S(2)}) copy-start(bf16[4,2,1152]{2,1,0:T(2,128)(2,1)} %param.27) | copy-start | bytes 55300
  30.4 15.0 %all-to-all-start = ((bf16[4,2,1536]{2,1,0:T(2,128)(2,1)}), bf16[4,2,1536]{2,1,0:T(2,128)(2,1)S(1)}, u32[]{:S(2)}, u32[]{:S(2)}) async-start(bf16[4,2,1536]{2,1,0:T(2,128)(2,1)} %reshape.441), calls=%async_computation | async-start | bytes 49152 | tf_op jit(solution)/shard_map/all_to_all | solution.py:112
  49.5 30.5 %copy-start.1 = (f32[2,1152]{1,0:T(2,128)S(1)}, f32[2,1152]{1,0:T(2,128)}, u32[]{:S(2)}) copy-start(f32[2,1152]{1,0:T(2,128)} %get-tuple-element.33) | copy-start | bytes 27652
  49.5 30.5 %copy-start.2 = (f32[2,1152]{1,0:T(2,128)S(1)}, f32[2,1152]{1,0:T(2,128)}, u32[]{:S(2)}) copy-start(f32[2,1152]{1,0:T(2,128)} %get-tuple-element.34) | copy-start | bytes 27652
  49.5 30.5 %copy-start.3 = (f32[2,1152]{1,0:T(2,128)S(1)}, f32[2,1152]{1,0:T(2,128)}, u32[]{:S(2)}) copy-start(f32[2,1152]{1,0:T(2,128)} %get-tuple-element.35) | copy-start | bytes 27652
  49.5 30.5 %copy-start.4 = (f32[2,1152]{1,0:T(2,128)S(1)}, f32[2,1152]{1,0:T(2,128)}, u32[]{:S(2)}) copy-start(f32[2,1152]{1,0:T(2,128)} %get-tuple-element.36) | copy-start | bytes 27652
  81.8 2.8 %copy-start.8 = (f32[32]{0:T(128)S(1)}, f32[32]{0:T(128)}, u32[]{:S(2)}) copy-start(f32[32]{0:T(128)} %param.26) | copy-start | bytes 388
  81.8 3.4 %copy-start.6 = (f32[2048]{0:T(1024)S(1)}, f32[2048]{0:T(1024)}, u32[]{:S(2)}) copy-start(f32[2048]{0:T(1024)} %param.32) | copy-start | bytes 24580
where the time goes:
time: 113 us
  blocking collectives  47 us (42%)
  other arithmetic  28.3 us (25%)
  local copies, waits for them, and re-layouts  18.6 us (16%)
  matrix products  11 us (10%)
  starting transfers between devices  6.35 us (6%)
  between operations  1.59 us (1%)
    unnamed x2, blocking collectives  33.9 us
    unnamed x1, other arithmetic  22.4 us
    all_gather x1, blocking collectives, local(): lax.all_gather(gate_applied_output, 'kv', axis=0, tiled=True)  13.1 us
    unnamed x25, local copies, waits for them, and re-layouts  10.4 us
    all_to_all x1, starting transfers between devices, local(): lax.all_to_all(normed, 'kv', split_axis=2, concat_axis=0, tiled=True)  6.35 us
    dot_general x1, matrix products, local(): jnp.einsum('sjd,dc->sjc', pieces, joined, preferred_element_type=jnp.floa...  4.97 us
    dot_general x1, matrix products, local(): jnp.einsum('sjc,cd->sjd', lax.all_gather(gate_applied_output, 'kv', axis=...  2.85 us
    convert_element_type x1, local copies, waits for them, and re-layouts, local(): (widened * rms_scale(widened) * input_norm_scale).astype(jnp.bfloat16)  2.84 us
  transfers between devices with their start and end apart: 1, of which 0 were waited for; matrix products, arithmetic and copies ran while one was open for 7% of the time, Pallas kernels for 0%

commit v1 on v0

--- a/solution.py
+++ b/solution.py
@@ -1,6 +1,10 @@
+import functools
+
 import jax
 import jax.numpy as jnp
 from jax import lax
+from jax.experimental import pallas as pl
+from jax.experimental.pallas import tpu as pltpu
 from jax.sharding import PartitionSpec as P
 
 epsilon = 1e-06
@@ -157,9 +161,495 @@
     return (mixed, running_state_rows, convolution_span)
 
 
+MESH_ID = pl.DeviceIdType.MESH
+
+
+def lane_chunks(width, piece):
+    return [(lo, min(piece, width - lo)) for lo in range(0, width, piece)]
+
+
+def split_rows(value):
+    high = value.astype(jnp.bfloat16).astype(jnp.float32)
+    rest = value - high
+    middle = rest.astype(jnp.bfloat16).astype(jnp.float32)
+    return high, middle, rest - middle
+
+
+def mixer_kernel(
+    sizes,
+    accepted,
+    tokens,
+    input_scale,
+    head_hbm,
+    gate_hbm,
+    inject_hbm,
+    readout_hbm,
+    step_hbm,
+    step_bias,
+    decay_rate,
+    direct_weight,
+    taps,
+    history,
+    states_hbm,
+    extra_decay,
+    norm_scale,
+    out_hbm,
+    mixed_out,
+    states_out,
+    tail_out,
+    head_w,
+    gate_w,
+    inject_w,
+    readout_w,
+    step_w,
+    states,
+    out_w,
+    normed_buf,
+    normed_in,
+    own_sum,
+    sum_buf,
+    sum_in,
+    gated_buf,
+    gated_in,
+    out_buf,
+    out_in,
+    span,
+    outer_buf,
+    decay_buf,
+    load_sem,
+    a_send,
+    a_recv,
+    b_send,
+    b_recv,
+    c_send,
+    c_recv,
+    d_send,
+    d_recv,
+):
+    kv, tp, rows, props = sizes
+    width = tokens.shape[-1]
+    part = width // kv
+    heads = step_bias.shape[-1]
+    groups, channels = taps.shape[1:]
+    head_dim, state = states.shape[2:]
+    per_group = heads // groups
+    inner = per_group * head_dim
+    inputs = heads * head_dim
+    bc = groups * state
+    taps_n = taps.shape[0]
+    f32 = jnp.float32
+    bf16 = jnp.bfloat16
+    me = lax.axis_index("kv")
+    me_tp = lax.axis_index("tp")
+
+    def kv_peer(d):
+        return lax.rem(me + d, kv)
+
+    def kv_source(d):
+        return lax.rem(me + kv - d, kv)
+
+    loads = []
+
+    def load(src, dst):
+        copy = pltpu.make_async_copy(src, dst, load_sem.at[len(loads)])
+        copy.start()
+        loads.append(copy)
+        return copy
+
+    step_load = load(step_hbm, step_w)
+    big = lane_chunks(inputs, inputs // 2)
+    head_loads = [load(head_hbm.at[:, lo : lo + n], head_w.at[:, lo : lo + n]) for lo, n in big]
+    group_loads = [load(inject_hbm, inject_w), load(readout_hbm, readout_w)]
+    gate_loads = [load(gate_hbm.at[:, lo : lo + n], gate_w.at[:, lo : lo + n]) for lo, n in big]
+    states_load = load(states_hbm.at[0], states)
+    out_load = load(out_hbm, out_w)
+
+    barrier = pltpu.get_barrier_semaphore()
+    for d in range(1, kv):
+        pl.semaphore_signal(barrier, 1, device_id={"kv": kv_peer(d)}, device_id_type=MESH_ID)
+    for d in range(1, tp):
+        pl.semaphore_signal(
+            barrier, 1, device_id={"tp": lax.rem(me_tp + d, tp)}, device_id_type=MESH_ID
+        )
+
+    wide = tokens[0].astype(f32)
+    normed = wide * rms_scale(wide) * input_scale[...]
+    normed = jnp.concatenate([normed, jnp.zeros((rows - props, width), f32)], axis=0)
+    for k in range(kv):
+        normed_buf[k] = normed[:, k * part : (k + 1) * part].astype(bf16)
+    pl.semaphore_wait(barrier, kv + tp - 2)
+
+    copies = []
+
+    def send(src, dst, send_sem, recv_sem, device):
+        copy = pltpu.make_async_remote_copy(
+            src_ref=src,
+            dst_ref=dst,
+            send_sem=send_sem,
+            recv_sem=recv_sem,
+            device_id=device,
+            device_id_type=MESH_ID,
+        )
+        copy.start()
+        copies.append(copy)
+        return copy
+
+    first = [
+        send(normed_buf.at[kv_peer(d)], normed_in.at[d], a_send.at[d], a_recv.at[d], {"kv": kv_peer(d)})
+        for d in range(1, kv)
+    ]
+
+    step_load.wait()
+    step_raw = lax.dot_general(
+        normed.astype(bf16), step_w[...], (((1,), (1,)), ((), ())), preferred_element_type=f32
+    )[:props]
+    biased = step_raw + step_bias[...]
+    step_size = jnp.maximum(biased, 0.0) + jnp.log1p(jnp.exp(-jnp.abs(biased)))
+    rate = jnp.exp(decay_rate[...])
+    log_rows = [extra_decay[j] - rate * step_size[j : j + 1] for j in range(props)]
+    cumulative = [log_rows[0]]
+    for j in range(1, props):
+        cumulative.append(cumulative[-1] + log_rows[j])
+    pairs = [(j, i) for j in range(props) for i in range(j + 1)]
+    stacked = [jnp.exp(row) for row in cumulative]
+    stacked += [jnp.exp(cumulative[j] - cumulative[i]) * step_size[i : i + 1] for j, i in pairs]
+    stacked.append(direct_weight[...])
+    count = len(stacked)
+    table = jnp.concatenate(stacked, axis=0)
+    padded = -(-3 * count // 16) * 16
+    pieces = list(split_rows(table)) + [jnp.zeros((padded - 3 * count, heads), f32)]
+    spread = (
+        lax.broadcasted_iota(jnp.int32, (heads, inputs), 1) // head_dim
+        == lax.broadcasted_iota(jnp.int32, (heads, inputs), 0)
+    )
+    wide_table = jnp.dot(
+        jnp.concatenate(pieces, axis=0).astype(bf16),
+        jnp.where(spread, 1.0, 0.0).astype(bf16),
+        preferred_element_type=f32,
+    )
+    expanded = wide_table[:count] + wide_table[count : 2 * count] + wide_table[2 * count : 3 * count]
+
+    dec = jnp.concatenate([jnp.exp(row) for row in log_rows], axis=0)
+    dec = jnp.concatenate([dec, jnp.zeros((8 - props, heads), f32)], axis=0)
+    dec = jnp.concatenate([dec, jnp.zeros((8, 128 - heads), f32)], axis=1)
+    dec_t = jnp.transpose(dec)
+    for j in range(props):
+        decay_buf[j] = jnp.broadcast_to(dec_t[:heads, j : j + 1], (heads, state))
+
+    start = jnp.maximum(accepted[0], 1)
+    for r in range(taps_n - 1):
+        row = history[0, start + r]
+        tail_out[0, r] = row
+        row = row.astype(f32)
+        for g in range(groups):
+            span[g, r : r + 1] = row[g : g + 1]
+
+    blocks = [normed_buf[me].astype(f32)]
+    for d in range(1, kv):
+        first[d - 1].wait_recv()
+        blocks.append(normed_in[d].astype(f32))
+    gathered = jnp.concatenate(blocks, axis=0).astype(bf16)
+
+    stages = []
+    for at, (lo, n) in enumerate(big):
+        stages.append((lo, [(head_w, lo, n)], [head_loads[at]]))
+    stages.append((inputs, [(inject_w, 0, bc), (readout_w, 0, bc)], group_loads))
+    for at, (lo, n) in enumerate(big):
+        stages.append((inputs + 2 * bc + lo, [(gate_w, lo, n)], [gate_loads[at]]))
+    second = [[] for _ in stages]
+    ranges = []
+
+    def send_sums(stage):
+        lo, n = ranges[stage]
+        for d in range(1, kv):
+            second[stage].append(
+                send(
+                    sum_buf.at[d, :, lo : lo + n],
+                    sum_in.at[d, :, lo : lo + n],
+                    b_send.at[stage, d],
+                    b_recv.at[stage, d],
+                    {"kv": kv_source(d)},
+                )
+            )
+
+    for stage, (base, operands, ready) in enumerate(stages):
+        for copy in ready:
+            copy.wait()
+        at = base
+        for ref, lo, n in operands:
+            for sub, size in lane_chunks(n, 512):
+                part_sum = jnp.dot(
+                    gathered, ref[:, lo + sub : lo + sub + size], preferred_element_type=f32
+                )
+                own_sum[:, at : at + size] = part_sum[:rows]
+                for d in range(1, kv):
+                    sum_buf[d, :, at : at + size] = part_sum[d * rows : (d + 1) * rows].astype(bf16)
+                at += size
+        ranges.append((base, at - base))
+        if stage:
+            send_sums(stage - 1)
+    states_load.wait()
+    send_sums(len(stages) - 1)
+
+    def summed(stage):
+        lo, n = ranges[stage]
+        total = own_sum[:, lo : lo + n]
+        for d in range(1, kv):
+            second[stage][d - 1].wait_recv()
+            total = total + sum_in[d, :, lo : lo + n].astype(f32)
+        return total.astype(bf16).astype(f32)[:props]
+
+    part_x = jnp.concatenate([summed(s) for s in range(len(big))], axis=1)
+    part_bc = summed(len(big))
+    fresh = []
+    for g in range(groups):
+        fresh.append(
+            jnp.concatenate(
+                [
+                    part_x[:, g * inner : (g + 1) * inner],
+                    part_bc[:, g * state : (g + 1) * state],
+                    part_bc[:, bc + g * state : bc + (g + 1) * state],
+                ],
+                axis=1,
+            )
+        )
+        span[g, taps_n - 1 : taps_n - 1 + props] = fresh[g]
+    for j in range(props):
+        tail_out[0, taps_n - 1 + j] = jnp.concatenate(
+            [fresh[g][j : j + 1] for g in range(groups)], axis=0
+        ).astype(bf16)
+
+    lhs_rows = [None] * groups
+    rhs = [None] * groups
+    responses = []
+    for g in range(groups):
+        conv = jnp.zeros((props, channels), f32)
+        for k in range(taps_n):
+            conv = conv + span[g, k : k + props] * taps[k].astype(f32)[g : g + 1]
+        act = conv * jax.nn.sigmoid(conv)
+        x = act[:, :inner]
+        b = act[:, inner : inner + state]
+        c = act[:, inner + state :]
+        cols = slice(g * inner, (g + 1) * inner)
+        previous = states[start - 1, g * per_group : (g + 1) * per_group].reshape(inner, state)
+        carried = lax.dot_general(
+            jnp.concatenate([c, jnp.zeros((16 - props, state), f32)], axis=0).astype(bf16),
+            previous.astype(bf16),
+            (((1,), (1,)), ((), ())),
+            preferred_element_type=f32,
+        )
+        out_rows = []
+        for j in range(props):
+            total = expanded[j : j + 1, cols] * carried[j : j + 1]
+            total = total + expanded[count - 1 : count, cols] * x[j : j + 1]
+            for i in range(j + 1):
+                weight = jnp.sum(b[i : i + 1] * c[j : j + 1], axis=-1, keepdims=True)
+                at = props + pairs.index((j, i))
+                total = total + expanded[at : at + 1, cols] * weight * x[i : i + 1]
+            out_rows.append(total)
+        responses.append(jnp.concatenate(out_rows, axis=0))
+        left, right = [], []
+        for j in range(props):
+            at = props + pairs.index((j, j))
+            scaled = expanded[at : at + 1, cols] * x[j : j + 1]
+            xh, xm, _ = split_rows(scaled)
+            bh, bm, _ = split_rows(b[j : j + 1])
+            left += [xh, xh, xm]
+            before = jnp.zeros((1, 128 * j), f32)
+            after = jnp.zeros((1, 128 * (props - j) - state), f32)
+            for row in (bh, bm, bh):
+                right.append(jnp.concatenate(([before] if j else []) + [row, after], axis=1))
+        extra = -len(left) % 16
+        lhs_rows[g] = jnp.concatenate(left + [jnp.zeros((extra, inner), f32)], axis=0)
+        rhs[g] = jnp.concatenate(right + [jnp.zeros((extra, 128 * props), f32)], axis=0)
+
+    gate = jnp.concatenate([summed(len(big) + 1 + s) for s in range(len(big))], axis=1)
+    for g in range(groups):
+        cols = slice(g * inner, (g + 1) * inner)
+        raw = gate[:, cols]
+        value = responses[g] * (raw * jax.nn.sigmoid(raw))
+        value = value * rms_scale(value) * norm_scale[:, cols]
+        value = jnp.concatenate([value, jnp.zeros((rows - props, inner), f32)], axis=0)
+        gated_buf[:, cols] = value.astype(bf16)
+
+    for g in range(groups):
+        outer_buf[g * inner : (g + 1) * inner] = jnp.dot(
+            jnp.transpose(lhs_rows[g]).astype(bf16), rhs[g].astype(bf16), preferred_element_type=f32
+        )
+        if g == 0:
+            third = [
+                send(gated_buf, gated_in.at[d], c_send.at[d], c_recv.at[d], {"kv": kv_peer(d)})
+                for d in range(1, kv)
+            ]
+
+    def head_step(h, _):
+        value = states[start - 1, h]
+        for j in range(props):
+            outer = outer_buf[pl.ds(pl.multiple_of(h * head_dim, head_dim), head_dim), 128 * j : 128 * j + state]
+            value = value * decay_buf[j, pl.ds(h, 1)] + outer
+            states_out[0, j, h] = value
+        return 0
+
+    lax.fori_loop(0, heads, head_step, 0, unroll=4)
+
+    out_load.wait()
+    blocks = [gated_buf[...].astype(f32)]
+    for d in range(1, kv):
+        third[d - 1].wait_recv()
+        blocks.append(gated_in[d].astype(f32))
+    everyone = jnp.concatenate(blocks, axis=0).astype(bf16)
+    fourth = []
+    for sub, size in lane_chunks(out_w.shape[1], 512):
+        product = jnp.dot(everyone, out_w[:, sub : sub + size], preferred_element_type=f32)
+        for d in range(kv):
+            out_buf[d, :, sub : sub + size] = product[d * rows : (d + 1) * rows].astype(bf16)
+    for d in range(1, tp):
+        target = lax.rem(me_tp + d, tp)
+        fourth.append(
+            send(
+                out_buf.at[lax.rem(me + kv - target, kv)],
+                out_in.at[d],
+                d_send.at[d],
+                d_recv.at[d],
+                {"tp": target},
+            )
+        )
+    total = out_buf[lax.rem(me + kv - me_tp, kv)].astype(f32)
+    for d in range(1, tp):
+        fourth[d - 1].wait_recv()
+        total = total + out_in[d].astype(f32)
+    mixed_out[0] = total[:props].astype(bf16)
+    for copy in copies:
+        copy.wait_send()
+
+
+def fused(kv, tp, args):
+    (
+        tokens,
+        input_norm_scale,
+        head_input_matrix,
+        output_gate_matrix,
+        group_input_matrix,
+        group_readout_matrix,
+        step_size_matrix,
+        step_size_bias,
+        log_decay_rate,
+        direct_path_weight,
+        convolution_tap_weight,
+        convolution_history_rows,
+        per_proposal_states,
+        accepted,
+        proposal_extra_decay,
+        group_norm_scale,
+        output_projection_matrix,
+    ) = args
+    _, props, width = tokens.shape
+    rows = -(-props // 4) * 4
+    heads = step_size_bias.shape[0]
+    groups, channels = convolution_tap_weight.shape[1:]
+    state = per_proposal_states.shape[4]
+    inputs = head_input_matrix.shape[1]
+    total = 2 * inputs + 2 * group_input_matrix.shape[1]
+    columns = output_projection_matrix.shape[1]
+    bf16, f32 = jnp.bfloat16, jnp.float32
+    stages = 5
+    vmem = pl.BlockSpec(memory_space=pltpu.VMEM)
+    hbm = pl.BlockSpec(memory_space=pl.ANY)
+    smem = pl.BlockSpec(memory_space=pltpu.SMEM)
+    dma = pltpu.SemaphoreType.DMA
+    return pl.pallas_call(
+        functools.partial(mixer_kernel, (kv, tp, rows, props)),
+        name="mixer",
+        out_shape=(
+            jax.ShapeDtypeStruct((1, props, columns), bf16),
+            jax.ShapeDtypeStruct(per_proposal_states.shape, f32),
+            jax.ShapeDtypeStruct(convolution_history_rows.shape, bf16),
+        ),
+        in_specs=[
+            smem, vmem, vmem, hbm, hbm, hbm, hbm, hbm,
+            vmem, vmem, vmem, vmem, vmem, hbm, vmem, vmem, hbm,
+        ],
+        out_specs=(vmem, vmem, vmem),
+        scratch_shapes=[
+            pltpu.VMEM(head_input_matrix.shape, bf16),
+            pltpu.VMEM(output_gate_matrix.shape, bf16),
+            pltpu.VMEM(group_input_matrix.shape, bf16),
+            pltpu.VMEM(group_readout_matrix.shape, bf16),
+            pltpu.VMEM(step_size_matrix.shape[::-1], bf16),
+            pltpu.VMEM(per_proposal_states.shape[1:], f32),
+            pltpu.VMEM(output_projection_matrix.shape, bf16),
+            pltpu.VMEM((kv, rows, width // kv), bf16),
+            pltpu.VMEM((kv, rows, width // kv), bf16),
+            pltpu.VMEM((rows, total), f32),
+            pltpu.VMEM((kv, rows, total), bf16),
+            pltpu.VMEM((kv, rows, total), bf16),
+            pltpu.VMEM((rows, inputs), bf16),
+            pltpu.VMEM((kv, rows, inputs), bf16),
+            pltpu.VMEM((kv, rows, columns), bf16),
+            pltpu.VMEM((tp, rows, columns), bf16),
+            pltpu.VMEM((groups, 8, channels), f32),
+            pltpu.VMEM((inputs, 128 * props), f32),
+            pltpu.VMEM((props, heads, state), f32),
+            dma((9,)),
+            dma((kv,)),
+            dma((kv,)),
+            dma((stages, kv)),
+            dma((stages, kv)),
+            dma((kv,)),
+            dma((kv,)),
+            dma((tp,)),
+            dma((tp,)),
+        ],
+        compiler_params=pltpu.CompilerParams(
+            collective_id=0, has_side_effects=True, vmem_limit_bytes=60 * 1024 * 1024
+        ),
+    )(
+        accepted,
+        tokens,
+        input_norm_scale[None],
+        head_input_matrix,
+        output_gate_matrix,
+        group_input_matrix,
+        group_readout_matrix,
+        step_size_matrix.T,
+        step_size_bias[None],
+        log_decay_rate[None],
+        direct_path_weight[None],
+        convolution_tap_weight,
+        convolution_history_rows,
+        per_proposal_states,
+        jnp.transpose(proposal_extra_decay, (1, 0, 2)),
+        group_norm_scale[None],
+        output_projection_matrix,
+    )
+
+
+def fits(kv, tp, args):
+    tokens, taps, states = args[0], args[10], args[12]
+    heads = args[7].shape[0]
+    slices = (tokens.shape[2] // kv, args[4].shape[1], args[16].shape[1])
+    return (
+        kv == tp
+        and tokens.shape[0] == 1
+        and tokens.shape[1] + taps.shape[0] - 1 <= 8
+        and heads <= 128
+        and states.shape[4] <= 128
+        and heads // taps.shape[1] * states.shape[3] % 128 == 0
+        and all(n % 128 == 0 for n in slices)
+        and args[2].shape[1] % 256 == 0
+    )
+
+
 def solution(mesh):
+    kv, tp = mesh.shape["kv"], mesh.shape["tp"]
+
+    def body(*args):
+        if fits(kv, tp, args):
+            return tuple(fused(kv, tp, args))
+        return local(*args)
+
     return jax.shard_map(
-        local,
+        body,
         mesh=mesh,
         in_specs=(
             P(("grp", "kv"), None, None),

time: 113 us -> 32 us (0.28)
  blocking collectives: 47 us -> 0 us
  other arithmetic: 28.3 us -> 0 us
  Pallas kernels: 0 us -> 24.5 us
  local copies, waits for them, and re-layouts: 18.6 us -> 5.89 us
  matrix products: 11 us -> 0 us
  starting transfers between devices: 6.35 us -> 0 us
    unnamed x2 -> x0, blocking collectives: 33.9 us -> none
    pallas_call x0 -> x1, Pallas kernels: none -> 24.5 us  [fused(): pl.pallas_call(functools.partial(mixer_kernel, (kv, tp, rows, props)), na...]
    unnamed x1 -> x0, other arithmetic: 22.4 us -> none
    all_gather x1 -> x0, blocking collectives: 13.1 us -> none  [local(): lax.all_gather(gate_applied_output, 'kv', axis=0, tiled=True)]
    dot_general x5 -> x0, matrix products: 11 us -> none  [the longest x1 4.97 us: local(): jnp.einsum('sjd,dc->sjc', pieces, joined, preferred_element_type=jnp.floa...]
    all_to_all x1 -> x0, starting transfers between devices: 6.35 us -> none  [local(): lax.all_to_all(normed, 'kv', split_axis=2, concat_axis=0, tiled=True)]
    unnamed x25 -> x5, local copies, waits for them, and re-layouts: 10.4 us -> 5.89 us
    convert_element_type x3 -> x0, local copies, waits for them, and re-layouts: 3.57 us -> none  [the longest x1 2.84 us: local(): (widened * rms_scale(widened) * input_norm_scale).astype(jnp.bfloat16)]
  transfers between devices with their start and end apart: 1 -> 0, of which waited for: 0 -> 0; matrix products, arithmetic and copies ran while one was open for 7% -> 0% of each run, Pallas kernels for 0% -> 0%
where the time goes in v1:
time: 32 us; the launch traced here: 31.7 us
  Pallas kernels  24.5 us (77%)
  local copies, waits for them, and re-layouts  5.89 us (18%)
  between operations  1.3 us (4%)
    pallas_call x1, Pallas kernels, fused(): pl.pallas_call(functools.partial(mixer_kernel, (kv, tp, rows, props)), na...  24.5 us
    unnamed x5, local copies, waits for them, and re-layouts  5.89 us

profile of v1, /device:TPU:0, one launch (start us, length us, event | category | flops | bytes accessed | tf_op | source)
XLA Modules:
  0.0 31.7 jit_solution(15753183874765713641)
XLA Ops:
  1.3 24.5 %mixer.1 = (bf16[1,3,1024]{2,1,0:T(4,128)(2,1)}, f32[1,3,32,64,64]{4,3,2,1,0:T(8,128)}, bf16[1,6,2,1152]{3,2,1,0:T(2,128)(2,1)}) custom-call(s32[1]{0:T(128)S(6)} %copy.23.accepted, bf16[1,3,4096]{2,1,0:T(4,128)(2,1)} %tokens.1, f32[1,4096]{1,0:T(1,128)} %bitcast.8, bf16[1024,2048]{1,0:T(8,128)(2,1)} %head_hbm.1, bf16[1024,2048]{1,0:T(8,128)(2,1)} %gate_hbm.1, ...), custom_call_target="tpu_custom_call" | custom-call | tf_op jit(solution)/shard_map/mixer/pallas_call | solution.py:560
  25.8 0.0 copy-start
  25.8 1.3 %copy.24 = bf16[1,3,1024]{2,1,0:T(4,128)(2,1)} copy(bf16[1,3,1024]{2,1,0:T(4,128)(2,1)} %get-tuple-element.6) | data formatting | bytes 12288
  27.1 4.0 %copy.25 = f32[1,3,32,64,64]{4,3,2,1,0:T(8,128)} copy(f32[1,3,32,64,64]{4,3,2,1,0:T(8,128)} %get-tuple-element.7) | data formatting | bytes 3145728
  31.1 0.0 copy-done
  31.1 0.6 %copy.26 = bf16[1,6,2,1152]{3,2,1,0:T(2,128)(2,1)} copy(bf16[1,6,2,1152]{3,2,1,0:T(2,128)(2,1)S(1)} %copy-done) | data formatting | bytes 55296
Async XLA Ops:
  25.8 5.3 %copy-start = (bf16[1,6,2,1152]{3,2,1,0:T(2,128)(2,1)S(1)}, bf16[1,6,2,1152]{3,2,1,0:T(2,128)(2,1)}, u32[]{:S(2)}) copy-start(bf16[1,6,2,1152]{3,2,1,0:T(2,128)(2,1)} %get-tuple-element.8) | copy-start | bytes 82948

commit v2 on v1

--- a/solution.py
+++ b/solution.py
@@ -178,25 +178,34 @@
 def mixer_kernel(
     sizes,
     accepted,
-    tokens,
-    input_scale,
+    tokens_hbm,
+    input_scale_hbm,
     head_hbm,
     gate_hbm,
     inject_hbm,
     readout_hbm,
     step_hbm,
+    step_bias_hbm,
+    decay_rate_hbm,
+    direct_weight_hbm,
+    taps_hbm,
+    history_hbm,
+    states_hbm,
+    extra_decay_hbm,
+    norm_scale_hbm,
+    out_hbm,
+    mixed_out,
+    states_out,
+    tail_out,
+    tokens,
+    input_scale,
     step_bias,
     decay_rate,
     direct_weight,
     taps,
     history,
-    states_hbm,
     extra_decay,
     norm_scale,
-    out_hbm,
-    mixed_out,
-    states_out,
-    tail_out,
     head_w,
     gate_w,
     inject_w,
@@ -248,22 +257,6 @@
     def kv_source(d):
         return lax.rem(me + kv - d, kv)
 
-    loads = []
-
-    def load(src, dst):
-        copy = pltpu.make_async_copy(src, dst, load_sem.at[len(loads)])
-        copy.start()
-        loads.append(copy)
-        return copy
-
-    step_load = load(step_hbm, step_w)
-    big = lane_chunks(inputs, inputs // 2)
-    head_loads = [load(head_hbm.at[:, lo : lo + n], head_w.at[:, lo : lo + n]) for lo, n in big]
-    group_loads = [load(inject_hbm, inject_w), load(readout_hbm, readout_w)]
-    gate_loads = [load(gate_hbm.at[:, lo : lo + n], gate_w.at[:, lo : lo + n]) for lo, n in big]
-    states_load = load(states_hbm.at[0], states)
-    out_load = load(out_hbm, out_w)
-
     barrier = pltpu.get_barrier_semaphore()
     for d in range(1, kv):
         pl.semaphore_signal(barrier, 1, device_id={"kv": kv_peer(d)}, device_id_type=MESH_ID)
@@ -272,6 +265,36 @@
             barrier, 1, device_id={"tp": lax.rem(me_tp + d, tp)}, device_id_type=MESH_ID
         )
 
+    loads = []
+
+    def load(src, dst):
+        copy = pltpu.make_async_copy(src, dst, load_sem.at[len(loads)])
+        copy.start()
+        loads.append(copy)
+        return copy
+
+    token_loads = [load(tokens_hbm, tokens), load(input_scale_hbm, input_scale)]
+    step_loads = [
+        load(step_hbm, step_w),
+        load(step_bias_hbm, step_bias),
+        load(decay_rate_hbm, decay_rate),
+        load(direct_weight_hbm, direct_weight),
+        load(extra_decay_hbm, extra_decay),
+    ]
+    row_loads = [
+        load(history_hbm, history),
+        load(taps_hbm, taps),
+        load(norm_scale_hbm, norm_scale),
+    ]
+    big = lane_chunks(inputs, inputs // 2)
+    head_loads = [load(head_hbm.at[:, lo : lo + n], head_w.at[:, lo : lo + n]) for lo, n in big]
+    group_loads = [load(inject_hbm, inject_w), load(readout_hbm, readout_w)]
+    gate_loads = [load(gate_hbm.at[:, lo : lo + n], gate_w.at[:, lo : lo + n]) for lo, n in big]
+    states_load = load(states_hbm.at[0], states)
+    out_load = load(out_hbm, out_w)
+
+    for copy in token_loads:
+        copy.wait()
     wide = tokens[0].astype(f32)
     normed = wide * rms_scale(wide) * input_scale[...]
     normed = jnp.concatenate([normed, jnp.zeros((rows - props, width), f32)], axis=0)
@@ -299,7 +322,8 @@
         for d in range(1, kv)
     ]
 
-    step_load.wait()
+    for copy in step_loads:
+        copy.wait()
     step_raw = lax.dot_general(
         normed.astype(bf16), step_w[...], (((1,), (1,)), ((), ())), preferred_element_type=f32
     )[:props]
@@ -336,6 +360,8 @@
     for j in range(props):
         decay_buf[j] = jnp.broadcast_to(dec_t[:heads, j : j + 1], (heads, state))
 
+    for copy in row_loads:
+        copy.wait()
     start = jnp.maximum(accepted[0], 1)
     for r in range(taps_n - 1):
         row = history[0, start + r]
@@ -472,15 +498,15 @@
         value = jnp.concatenate([value, jnp.zeros((rows - props, inner), f32)], axis=0)
         gated_buf[:, cols] = value.astype(bf16)
 
+    third = [
+        send(gated_buf, gated_in.at[d], c_send.at[d], c_recv.at[d], {"kv": kv_peer(d)})
+        for d in range(1, kv)
+    ]
+
     for g in range(groups):
         outer_buf[g * inner : (g + 1) * inner] = jnp.dot(
             jnp.transpose(lhs_rows[g]).astype(bf16), rhs[g].astype(bf16), preferred_element_type=f32
         )
-        if g == 0:
-            third = [
-                send(gated_buf, gated_in.at[d], c_send.at[d], c_recv.at[d], {"kv": kv_peer(d)})
-                for d in range(1, kv)
-            ]
 
     def head_step(h, _):
         value = states[start - 1, h]
@@ -499,24 +525,31 @@
         blocks.append(gated_in[d].astype(f32))
     everyone = jnp.concatenate(blocks, axis=0).astype(bf16)
     fourth = []
-    for sub, size in lane_chunks(out_w.shape[1], 512):
-        product = jnp.dot(everyone, out_w[:, sub : sub + size], preferred_element_type=f32)
+    pieces = lane_chunks(out_w.shape[1], out_w.shape[1] // 2)
+
+    def send_out(piece):
+        lo, n = pieces[piece]
+        for d in range(1, tp):
+            target = lax.rem(me_tp + d, tp)
+            fourth.append(
+                send(
+                    out_buf.at[lax.rem(me + kv - target, kv), :, lo : lo + n],
+                    out_in.at[d, :, lo : lo + n],
+                    d_send.at[piece, d],
+                    d_recv.at[piece, d],
+                    {"tp": target},
+                )
+            )
+
+    for piece, (lo, n) in enumerate(pieces):
+        product = jnp.dot(everyone, out_w[:, lo : lo + n], preferred_element_type=f32)
         for d in range(kv):
-            out_buf[d, :, sub : sub + size] = product[d * rows : (d + 1) * rows].astype(bf16)
-    for d in range(1, tp):
-        target = lax.rem(me_tp + d, tp)
-        fourth.append(
-            send(
-                out_buf.at[lax.rem(me + kv - target, kv)],
-                out_in.at[d],
-                d_send.at[d],
-                d_recv.at[d],
-                {"tp": target},
-            )
-        )
+            out_buf[d, :, lo : lo + n] = product[d * rows : (d + 1) * rows].astype(bf16)
+        send_out(piece)
+    for copy in fourth:
+        copy.wait_recv()
     total = out_buf[lax.rem(me + kv - me_tp, kv)].astype(f32)
     for d in range(1, tp):
-        fourth[d - 1].wait_recv()
         total = total + out_in[d].astype(f32)
     mixed_out[0] = total[:props].astype(bf16)
     for copy in copies:
@@ -554,23 +587,28 @@
     bf16, f32 = jnp.bfloat16, jnp.float32
     stages = 5
     vmem = pl.BlockSpec(memory_space=pltpu.VMEM)
-    hbm = pl.BlockSpec(memory_space=pl.ANY)
-    smem = pl.BlockSpec(memory_space=pltpu.SMEM)
+    hbm = pl.BlockSpec(memory_space=pltpu.HBM)
     dma = pltpu.SemaphoreType.DMA
     return pl.pallas_call(
         functools.partial(mixer_kernel, (kv, tp, rows, props)),
         name="mixer",
         out_shape=(
-            jax.ShapeDtypeStruct((1, props, columns), bf16),
-            jax.ShapeDtypeStruct(per_proposal_states.shape, f32),
-            jax.ShapeDtypeStruct(convolution_history_rows.shape, bf16),
+            pltpu.VMEM((1, props, columns), bf16),
+            pltpu.VMEM(per_proposal_states.shape, f32),
+            pltpu.VMEM(convolution_history_rows.shape, bf16),
         ),
-        in_specs=[
-            smem, vmem, vmem, hbm, hbm, hbm, hbm, hbm,
-            vmem, vmem, vmem, vmem, vmem, hbm, vmem, vmem, hbm,
-        ],
+        in_specs=[pl.BlockSpec(memory_space=pltpu.SMEM)] + [hbm] * 16,
         out_specs=(vmem, vmem, vmem),
         scratch_shapes=[
+            pltpu.VMEM(tokens.shape, bf16),
+            pltpu.VMEM((1, width), f32),
+            pltpu.VMEM((1, heads), f32),
+            pltpu.VMEM((1, heads), f32),
+            pltpu.VMEM((1, heads), f32),
+            pltpu.VMEM(convolution_tap_weight.shape, bf16),
+            pltpu.VMEM(convolution_history_rows.shape, bf16),
+            pltpu.VMEM((props, 1, heads), f32),
+            pltpu.VMEM((1, inputs), f32),
             pltpu.VMEM(head_input_matrix.shape, bf16),
             pltpu.VMEM(output_gate_matrix.shape, bf16),
             pltpu.VMEM(group_input_matrix.shape, bf16),
@@ -590,37 +628,42 @@
             pltpu.VMEM((groups, 8, channels), f32),
             pltpu.VMEM((inputs, 128 * props), f32),
             pltpu.VMEM((props, heads, state), f32),
-            dma((9,)),
+            dma((19,)),
             dma((kv,)),
             dma((kv,)),
             dma((stages, kv)),
             dma((stages, kv)),
             dma((kv,)),
             dma((kv,)),
-            dma((tp,)),
-            dma((tp,)),
+            dma((2, tp)),
+            dma((2, tp)),
         ],
         compiler_params=pltpu.CompilerParams(
-            collective_id=0, has_side_effects=True, vmem_limit_bytes=60 * 1024 * 1024
+            collective_id=0, has_side_effects=True, vmem_limit_bytes=48 * 1024 * 1024
         ),
     )(
         accepted,
-        tokens,
-        input_norm_scale[None],
-        head_input_matrix,
-        output_gate_matrix,
-        group_input_matrix,
-        group_readout_matrix,
-        step_size_matrix.T,
-        step_size_bias[None],
-        log_decay_rate[None],
-        direct_path_weight[None],
-        convolution_tap_weight,
-        convolution_history_rows,
-        per_proposal_states,
-        jnp.transpose(proposal_extra_decay, (1, 0, 2)),
-        group_norm_scale[None],
-        output_projection_matrix,
+        *[
+            pltpu.with_memory_space_constraint(value, pltpu.HBM)
+            for value in (
+                tokens,
+                input_norm_scale[None],
+                head_input_matrix,
+                output_gate_matrix,
+                group_input_matrix,
+                group_readout_matrix,
+                step_size_matrix.T,
+                step_size_bias[None],
+                log_decay_rate[None],
+                direct_path_weight[None],
+                convolution_tap_weight,
+                convolution_history_rows,
+                per_proposal_states,
+                jnp.transpose(proposal_extra_decay, (1, 0, 2)),
+                group_norm_scale[None],
+                output_projection_matrix,
+            )
+        ]
     )
 
 
@@ -635,7 +678,7 @@
         and heads <= 128
         and states.shape[4] <= 128
         and heads // taps.shape[1] * states.shape[3] % 128 == 0
-        and all(n % 128 == 0 for n in slices)
+        and all(n % 256 == 0 or n == slices[1] and n % 128 == 0 for n in slices)
         and args[2].shape[1] % 256 == 0
     )
 

time: 32 us -> 26.5 us (0.83)
  local copies, waits for them, and re-layouts: 5.89 us -> 2.87 us
  Pallas kernels: 24.5 us -> 22.2 us
    unnamed x5 -> x3, local copies, waits for them, and re-layouts: 5.89 us -> 2.87 us
    pallas_call x1, Pallas kernels: 24.5 us -> 22.2 us  [fused(): pl.pallas_call(functools.partial(mixer_kernel, (kv, tp, rows, props)), na...]
where the time goes in v2:
time: 26.5 us; the launch traced here: 26.3 us
  Pallas kernels  22.2 us (84%)
  local copies, waits for them, and re-layouts  2.87 us (11%)
  between operations  1.29 us (5%)
    pallas_call x1, Pallas kernels, fused(): pl.pallas_call(functools.partial(mixer_kernel, (kv, tp, rows, props)), na...  22.2 us
    unnamed x3, local copies, waits for them, and re-layouts  2.87 us

profile of v2, /device:TPU:0, one launch (start us, length us, event | category | flops | bytes accessed | tf_op | source)
XLA Modules:
  0.0 26.3 jit_solution(17089839948102020919)
XLA Ops:
  1.3 22.2 %mixer.1 = (bf16[1,3,1024]{2,1,0:T(4,128)(2,1)S(1)}, f32[1,3,32,64,64]{4,3,2,1,0:T(8,128)S(1)}, bf16[1,6,2,1152]{3,2,1,0:T(2,128)(2,1)S(1)}) custom-call(s32[1]{0:T(128)S(6)} %copy.26.accepted, bf16[1,3,4096]{2,1,0:T(4,128)(2,1)} %tokens_hbm.1, f32[1,4096]{1,0:T(1,128)} %bitcast.8, bf16[1024,2048]{1,0:T(8,128)(2,1)} %head_hbm.1, ...), custom_call_target="tpu_custom_call" | custom-call | tf_op jit(solution)/shard_map/mixer/pallas_call | solution.py:592
  23.5 0.6 %copy.23 = bf16[1,3,1024]{2,1,0:T(4,128)(2,1)} copy(bf16[1,3,1024]{2,1,0:T(4,128)(2,1)S(1)} %get-tuple-element.3) | data formatting | bytes 12288
  24.1 0.6 %copy.25 = bf16[1,6,2,1152]{3,2,1,0:T(2,128)(2,1)} copy(bf16[1,6,2,1152]{3,2,1,0:T(2,128)(2,1)S(1)} %get-tuple-element.5) | data formatting | bytes 55296
  24.7 1.7 %copy.24 = f32[1,3,32,64,64]{4,3,2,1,0:T(8,128)} copy(f32[1,3,32,64,64]{4,3,2,1,0:T(8,128)S(1)} %get-tuple-element.4) | data formatting | bytes 3145728

commit v3 on v2

--- a/solution.py
+++ b/solution.py
@@ -286,9 +286,9 @@
         load(taps_hbm, taps),
         load(norm_scale_hbm, norm_scale),
     ]
-    big = lane_chunks(inputs, inputs // 2)
+    big = lane_chunks(inputs, inner)
+    group_loads = [load(inject_hbm, inject_w), load(readout_hbm, readout_w)]
     head_loads = [load(head_hbm.at[:, lo : lo + n], head_w.at[:, lo : lo + n]) for lo, n in big]
-    group_loads = [load(inject_hbm, inject_w), load(readout_hbm, readout_w)]
     gate_loads = [load(gate_hbm.at[:, lo : lo + n], gate_w.at[:, lo : lo + n]) for lo, n in big]
     states_load = load(states_hbm.at[0], states)
     out_load = load(out_hbm, out_w)
@@ -376,10 +376,9 @@
         blocks.append(normed_in[d].astype(f32))
     gathered = jnp.concatenate(blocks, axis=0).astype(bf16)
 
-    stages = []
+    stages = [(inputs, [(inject_w, 0, bc), (readout_w, 0, bc)], group_loads)]
     for at, (lo, n) in enumerate(big):
         stages.append((lo, [(head_w, lo, n)], [head_loads[at]]))
-    stages.append((inputs, [(inject_w, 0, bc), (readout_w, 0, bc)], group_loads))
     for at, (lo, n) in enumerate(big):
         stages.append((inputs + 2 * bc + lo, [(gate_w, lo, n)], [gate_loads[at]]))
     second = [[] for _ in stages]
@@ -425,14 +424,13 @@
             total = total + sum_in[d, :, lo : lo + n].astype(f32)
         return total.astype(bf16).astype(f32)[:props]
 
-    part_x = jnp.concatenate([summed(s) for s in range(len(big))], axis=1)
-    part_bc = summed(len(big))
-    fresh = []
+    part_bc = summed(0)
+    fresh, xs, bs, responses = [], [], [], []
     for g in range(groups):
         fresh.append(
             jnp.concatenate(
                 [
-                    part_x[:, g * inner : (g + 1) * inner],
+                    summed(1 + g),
                     part_bc[:, g * state : (g + 1) * state],
                     part_bc[:, bc + g * state : bc + (g + 1) * state],
                 ],
@@ -440,15 +438,6 @@
             )
         )
         span[g, taps_n - 1 : taps_n - 1 + props] = fresh[g]
-    for j in range(props):
-        tail_out[0, taps_n - 1 + j] = jnp.concatenate(
-            [fresh[g][j : j + 1] for g in range(groups)], axis=0
-        ).astype(bf16)
-
-    lhs_rows = [None] * groups
-    rhs = [None] * groups
-    responses = []
-    for g in range(groups):
         conv = jnp.zeros((props, channels), f32)
         for k in range(taps_n):
             conv = conv + span[g, k : k + props] * taps[k].astype(f32)[g : g + 1]
@@ -456,6 +445,8 @@
         x = act[:, :inner]
         b = act[:, inner : inner + state]
         c = act[:, inner + state :]
+        xs.append(x)
+        bs.append(b)
         cols = slice(g * inner, (g + 1) * inner)
         previous = states[start - 1, g * per_group : (g + 1) * per_group].reshape(inner, state)
         carried = lax.dot_general(
@@ -474,38 +465,49 @@
                 total = total + expanded[at : at + 1, cols] * weight * x[i : i + 1]
             out_rows.append(total)
         responses.append(jnp.concatenate(out_rows, axis=0))
+
+    third = []
+    for g in range(groups):
+        cols = slice(g * inner, (g + 1) * inner)
+        raw = summed(1 + groups + g)
+        value = responses[g] * (raw * jax.nn.sigmoid(raw))
+        value = value * rms_scale(value) * norm_scale[:, cols]
+        value = jnp.concatenate([value, jnp.zeros((rows - props, inner), f32)], axis=0)
+        gated_buf[:, cols] = value.astype(bf16)
+        third.append(
+            [
+                send(
+                    gated_buf.at[:, cols],
+                    gated_in.at[d, :, cols],
+                    c_send.at[g, d],
+                    c_recv.at[g, d],
+                    {"kv": kv_peer(d)},
+                )
+                for d in range(1, kv)
+            ]
+        )
+
+    for j in range(props):
+        tail_out[0, taps_n - 1 + j] = jnp.concatenate(
+            [fresh[g][j : j + 1] for g in range(groups)], axis=0
+        ).astype(bf16)
+    for g in range(groups):
+        cols = slice(g * inner, (g + 1) * inner)
         left, right = [], []
         for j in range(props):
             at = props + pairs.index((j, j))
-            scaled = expanded[at : at + 1, cols] * x[j : j + 1]
-            xh, xm, _ = split_rows(scaled)
-            bh, bm, _ = split_rows(b[j : j + 1])
+            xh, xm, _ = split_rows(expanded[at : at + 1, cols] * xs[g][j : j + 1])
+            bh, bm, _ = split_rows(bs[g][j : j + 1])
             left += [xh, xh, xm]
             before = jnp.zeros((1, 128 * j), f32)
             after = jnp.zeros((1, 128 * (props - j) - state), f32)
             for row in (bh, bm, bh):
                 right.append(jnp.concatenate(([before] if j else []) + [row, after], axis=1))
         extra = -len(left) % 16
-        lhs_rows[g] = jnp.concatenate(left + [jnp.zeros((extra, inner), f32)], axis=0)
-        rhs[g] = jnp.concatenate(right + [jnp.zeros((extra, 128 * props), f32)], axis=0)
-
-    gate = jnp.concatenate([summed(len(big) + 1 + s) for s in range(len(big))], axis=1)
-    for g in range(groups):
-        cols = slice(g * inner, (g + 1) * inner)
-        raw = gate[:, cols]
-        value = responses[g] * (raw * jax.nn.sigmoid(raw))
-        value = value * rms_scale(value) * norm_scale[:, cols]
-        value = jnp.concatenate([value, jnp.zeros((rows - props, inner), f32)], axis=0)
-        gated_buf[:, cols] = value.astype(bf16)
-
-    third = [
-        send(gated_buf, gated_in.at[d], c_send.at[d], c_recv.at[d], {"kv": kv_peer(d)})
-        for d in range(1, kv)
-    ]
-
-    for g in range(groups):
-        outer_buf[g * inner : (g + 1) * inner] = jnp.dot(
-            jnp.transpose(lhs_rows[g]).astype(bf16), rhs[g].astype(bf16), preferred_element_type=f32
+        left = jnp.concatenate(left + [jnp.zeros((extra, inner), f32)], axis=0)
+        right = jnp.concatenate(right + [jnp.zeros((extra, 128 * props), f32)], axis=0)
+        outer_buf[cols] = jnp.dot(
+            jnp.transpose(left).astype(bf16), right.astype(bf16), preferred_element_type=f32
         )
 
     def head_step(h, _):
@@ -519,11 +521,15 @@
     lax.fori_loop(0, heads, head_step, 0, unroll=4)
 
     out_load.wait()
-    blocks = [gated_buf[...].astype(f32)]
-    for d in range(1, kv):
-        third[d - 1].wait_recv()
-        blocks.append(gated_in[d].astype(f32))
-    everyone = jnp.concatenate(blocks, axis=0).astype(bf16)
+    everyone = []
+    for g in range(groups):
+        cols = slice(g * inner, (g + 1) * inner)
+        blocks = [gated_buf[:, cols].astype(f32)]
+        for d in range(1, kv):
+            third[g][d - 1].wait_recv()
+            blocks.append(gated_in[d, :, cols].astype(f32))
+        everyone.append(jnp.concatenate(blocks, axis=0).astype(bf16))
+    everyone = jnp.concatenate(everyone, axis=1)
     fourth = []
     pieces = lane_chunks(out_w.shape[1], out_w.shape[1] // 2)
 
@@ -585,11 +591,11 @@
     total = 2 * inputs + 2 * group_input_matrix.shape[1]
     columns = output_projection_matrix.shape[1]
     bf16, f32 = jnp.bfloat16, jnp.float32
-    stages = 5
+    stages = 1 + 2 * groups
     vmem = pl.BlockSpec(memory_space=pltpu.VMEM)
     hbm = pl.BlockSpec(memory_space=pltpu.HBM)
     dma = pltpu.SemaphoreType.DMA
-    return pl.pallas_call(
+    results = pl.pallas_call(
         functools.partial(mixer_kernel, (kv, tp, rows, props)),
         name="mixer",
         out_shape=(
@@ -628,13 +634,13 @@
             pltpu.VMEM((groups, 8, channels), f32),
             pltpu.VMEM((inputs, 128 * props), f32),
             pltpu.VMEM((props, heads, state), f32),
-            dma((19,)),
+            dma((14 + 2 * groups,)),
             dma((kv,)),
             dma((kv,)),
             dma((stages, kv)),
             dma((stages, kv)),
-            dma((kv,)),
-            dma((kv,)),
+            dma((groups, kv)),
+            dma((groups, kv)),
             dma((2, tp)),
             dma((2, tp)),
         ],
@@ -665,6 +671,29 @@
             )
         ]
     )
+    return pl.pallas_call(
+        place_kernel,
+        name="place",
+        out_shape=tuple(jax.ShapeDtypeStruct(r.shape, r.dtype) for r in results),
+        in_specs=[vmem] * 3,
+        out_specs=(hbm, hbm, hbm),
+        scratch_shapes=[dma((2 + props,))],
+    )(*[pltpu.with_memory_space_constraint(value, pltpu.VMEM) for value in results])
+
+
+def place_kernel(*refs):
+    sems = refs[-1]
+    sources, targets = refs[:3], refs[3:6]
+    copies = []
+    for source, target in zip(sources, targets):
+        parts = range(source.shape[1]) if len(source.shape) == 5 else [None]
+        for part in parts:
+            view = (lambda ref: ref) if part is None else (lambda ref: ref.at[:, part])
+            copy = pltpu.make_async_copy(view(source), view(target), sems.at[len(copies)])
+            copy.start()
+            copies.append(copy)
+    for copy in copies:
+        copy.wait()
 
 
 def fits(kv, tp, args):

time: 26.5 us -> 25.5 us (0.962)
  local copies, waits for them, and re-layouts: 2.87 us -> 0 us
  Pallas kernels: 22.2 us -> 24 us
    unnamed x3 -> x0, local copies, waits for them, and re-layouts: 2.87 us -> none
    pallas_call x0 -> x1, Pallas kernels: none -> 1.71 us  [fused(): pl.pallas_call(place_kernel, name='place', out_shape=tuple((jax.ShapeDtyp...]
where the time goes in v3:
time: 25.5 us; the launch traced here: 25.3 us
  Pallas kernels  24 us (94%)
  between operations  1.29 us (5%)
    pallas_call x1, Pallas kernels, fused(): pl.pallas_call(functools.partial(mixer_kernel, (kv, tp, rows, props)), na...  22.3 us
    pallas_call x1, Pallas kernels, fused(): pl.pallas_call(place_kernel, name='place', out_shape=tuple((jax.ShapeDtyp...  1.71 us

profile of v3, /device:TPU:0, one launch (start us, length us, event | category | flops | bytes accessed | tf_op | source)
XLA Modules:
  0.0 25.3 jit_solution(3135590497379687026)
XLA Ops:
  1.3 22.3 %mixer.1 = (bf16[1,3,1024]{2,1,0:T(4,128)(2,1)S(1)}, f32[1,3,32,64,64]{4,3,2,1,0:T(8,128)S(1)}, bf16[1,6,2,1152]{3,2,1,0:T(2,128)(2,1)S(1)}) custom-call(s32[1]{0:T(128)S(6)} %copy.20.accepted, bf16[1,3,4096]{2,1,0:T(4,128)(2,1)} %tokens_hbm.1, f32[1,4096]{1,0:T(1,128)} %bitcast.8, bf16[1024,2048]{1,0:T(8,128)(2,1)} %head_hbm.1, ...), custom_call_target="tpu_custom_call" | custom-call | tf_op jit(solution)/shard_map/mixer/pallas_call | solution.py:598
  23.6 1.7 %place.1 = (bf16[1,3,1024]{2,1,0:T(4,128)(2,1)}, f32[1,3,32,64,64]{4,3,2,1,0:T(8,128)}, bf16[1,6,2,1152]{3,2,1,0:T(2,128)(2,1)}) custom-call(bf16[1,3,1024]{2,1,0:T(4,128)(2,1)S(1)} %get-tuple-element.6.refs_0_, f32[1,3,32,64,64]{4,3,2,1,0:T(8,128)S(1)} %get-tuple-element.7.refs_1_, bf16[1,6,2,1152]{3,2,1,0:T(2,128)(2,1)S(1)} %get-tuple-element.8.refs_2_), custom_call_target="tpu_custom_call" | custom-call | tf_op jit(solution)/shard_map/place/pallas_call | solution.py:674
